TPU v7x, 32 devices: a whole 2x2x4 slice. The times are simulated.
32 devices in a mesh: dp: 4 (over y, x), kv: 4 (over z), tp: 2 (over core).
Axes of the slice: x: 2, y: 2, z: 4, core: 2. Of those that a mesh axis runs over, the one named last changes fastest.
Arguments:
- tokens: bfloat16 [16, 4096], P('dp', 'kv'), may hold values from -18 to 18
- norm_gain: float32 [4096], P('kv'), may hold values from 0.1 to 1.9
- query_weight: bfloat16 [4096, 4096], P('kv', 'tp'), may hold values from -0.09375 to 0.09375
- key_weight: bfloat16 [4096, 512], P('kv', 'tp'), may hold values from -0.09375 to 0.09375
- value_weight: bfloat16 [4096, 512], P('kv', 'tp'), may hold values from -0.09375 to 0.09375
- gate_weight: bfloat16 [4096, 8], replicated, may hold values from -0.09375 to 0.09375
- gate_bias: float32 [8], replicated, may hold values from -2.5 to 0.5
- query_gain: float32 [64], replicated, may hold values from 0.1 to 1.9
- key_gain: float32 [64], replicated, may hold values from 0.1 to 1.9
- key_cache: bfloat16 [16, 8192, 512], P('dp', 'kv', 'tp'), may hold values from -6 to 6
- value_cache: bfloat16 [16, 8192, 512], P('dp', 'kv', 'tp'), may hold values from -9 to 9
- gate_cache: float32 [16, 8, 8192], P('dp', 'tp', 'kv'), may hold values from -8192 to 0, as said below
- lengths: int32 [16], P('dp'), may hold values from 4097 to 8192, as said below
- out_weight: bfloat16 [4096, 4096], P('tp', 'kv'), may hold values from -0.75 to 0.75
Outputs:
- mixed: bfloat16 [16, 4096], P('dp', 'kv')
Inputs may be any that keep to these rules, and one draw needn't show every extreme that they name: `gate_cache`: never rising along positions. `lengths`: in every draw some sequence has all 8192 positions cached.
All inputs are finite; a program needn't handle non-finite values.
Results may differ from a plain program's by a relative error of at most 0.012.
Values may be sent and summed in bfloat16 or wider, within the bound.
A program may use at most 64 MiB of HBM per device.

v0:
```python
import jax
import jax.numpy as jnp
from jax import lax
from jax.sharding import PartitionSpec as P

D = 4096
HEADS = 64
KV_HEADS = 8
HEAD = 64


EPSILON = 1e-06
FLOOR = -1e30


def head_norm(values, gain):
    values = values.astype(jnp.float32)
    return values * lax.rsqrt(jnp.mean(values * values, axis=-1, keepdims=True) + EPSILON) * gain


def per_device(
    tokens,
    norm_gain,
    query_weight,
    key_weight,
    value_weight,
    gate_weight,
    gate_bias,
    query_gain,
    key_gain,
    key_cache,
    value_cache,
    gate_cache,
    lengths,
    out_weight,
):
    seqs, columns = tokens.shape
    kv_rank = lax.axis_index("kv")
    tp_rank = lax.axis_index("tp")
    key_width = key_weight.shape[1]
    groups = key_width // HEAD
    ratio = HEADS // KV_HEADS
    positions = key_cache.shape[1]
    tokens_f = tokens.astype(jnp.float32)
    squares = jnp.sum(tokens_f * tokens_f, axis=1)
    scaled = (tokens_f * norm_gain).astype(jnp.bfloat16)
    query_part = jnp.dot(scaled, query_weight, preferred_element_type=jnp.float32)
    key_part = jnp.dot(scaled, key_weight, preferred_element_type=jnp.float32)
    value_part = jnp.dot(scaled, value_weight, preferred_element_type=jnp.float32)
    gate_rows = lax.dynamic_slice(
        gate_weight, (kv_rank * columns, tp_rank * groups), (columns, groups)
    )
    gate_part = jnp.dot(scaled, gate_rows, preferred_element_type=jnp.float32)
    query_sum, key_sum, value_sum, gate_sum, square_sum = lax.psum(
        (query_part, key_part, value_part, gate_part, squares), "kv"
    )
    inverse = lax.rsqrt(square_sum / D + EPSILON)[:, None]
    query_raw = (query_sum * inverse).astype(jnp.bfloat16)
    key_raw = (key_sum * inverse).astype(jnp.bfloat16)
    value_raw = (value_sum * inverse).astype(jnp.bfloat16)
    local_bias = lax.dynamic_slice_in_dim(gate_bias, tp_rank * groups, groups)
    log_gate = jax.nn.log_sigmoid(gate_sum * inverse + local_bias)
    queries = head_norm(query_raw.reshape(seqs, groups, ratio, HEAD), query_gain).astype(
        jnp.bfloat16
    )
    key_new = head_norm(key_raw.reshape(seqs, groups, HEAD), key_gain).astype(jnp.bfloat16)
    value_new = value_raw.reshape(seqs, groups, HEAD).astype(jnp.float32)
    keys = key_cache.reshape(seqs, positions, groups, HEAD)
    values = value_cache.reshape(seqs, positions, groups, HEAD)
    scale = HEAD ** (-0.5)
    scores = (
        jnp.einsum("sgrd,spgd->sgrp", queries, keys, preferred_element_type=jnp.float32) * scale
    )
    scores = scores - gate_cache[:, :, None, :]
    offsets = jnp.arange(positions, dtype=jnp.int32)
    live = ((kv_rank * positions + offsets)[None, :] < lengths[:, None])[:, None, None, :]
    within = lengths - 1 - kv_rank * positions
    owner = ((within >= 0) & (within < positions))[:, None, None]
    picked = (offsets[None, :] == within[:, None])[:, None, :]
    last_gate = jnp.sum(jnp.where(picked, gate_cache, 0.0), axis=2)
    own_gate = last_gate + log_gate
    score_new = (
        jnp.einsum("sgrd,sgd->sgr", queries, key_new, preferred_element_type=jnp.float32) * scale
    )
    score_new = score_new - own_gate[:, :, None]
    maxima = jnp.max(jnp.where(live, scores, FLOOR), axis=3)
    maxima = jnp.where(owner, jnp.maximum(maxima, score_new), maxima)
    weights = jnp.where(live, jnp.exp(scores - maxima[..., None]), 0.0).astype(jnp.bfloat16)
    weight_new = (
        jnp.where(owner, jnp.exp(score_new - maxima), 0.0).astype(jnp.bfloat16).astype(jnp.float32)
    )
    totals = jnp.sum(weights.astype(jnp.float32), axis=3) + weight_new
    weighted = jnp.einsum("sgrp,spgd->sgrd", weights, values, preferred_element_type=jnp.float32)
    weighted = weighted + weight_new[..., None] * value_new[:, :, None, :]
    top = lax.pmax(maxima, "kv")
    factor = jnp.exp(maxima - top)
    total, summed = lax.psum((totals * factor, weighted * factor[..., None]), "kv")
    attended = (summed / total[..., None]).astype(jnp.bfloat16).reshape(seqs, groups * ratio * HEAD)
    partial_value = jnp.dot(attended, out_weight, preferred_element_type=jnp.float32).astype(
        jnp.bfloat16
    )
    partial_value = lax.optimization_barrier(partial_value).astype(jnp.float32)
    return lax.psum(partial_value.astype(jnp.bfloat16), "tp")


def solution(mesh):
    return jax.shard_map(
        per_device,
        mesh=mesh,
        in_specs=(
            P("dp", "kv"),
            P("kv"),
            P("kv", "tp"),
            P("kv", "tp"),
            P("kv", "tp"),
            P(),
            P(),
            P(),
            P(),
            P("dp", "kv", "tp"),
            P("dp", "kv", "tp"),
            P("dp", "tp", "kv"),
            P("dp"),
            P("tp", "kv"),
        ),
        out_specs=P("dp", "kv"),
        check_vma=False,
    )
```

profile of v0, /device:TPU:0, one launch (start us, length us, event | category | flops | bytes accessed | tf_op | source)
XLA Modules:
  0.0 85.6 jit_solution(17493056024929057668)
XLA Ops:
  0.0 0.8 dynamic_slice.7
  0.8 0.8 fusion.3
  1.6 0.9 %fusion.5 = f32[4,4]{1,0:T(4,128)S(1)} fusion(bf16[4096,8]{0,1:T(8,128)(2,1)} %param.19, s32[]{:T(128)S(6)} %select_n.33, s32[]{:T(128)S(6)} %select_n.34, bf16[4,1024]{1,0:T(4,128)(2,1)} %param.14, f32[1024]{0:T(1024)} %param.15), kind=kOutput, calls=%fused_computation.29 | convolution fusion | flops 45056 | bytes 20552 | tf_op jit(solution)/shard_map/dot_general | solution.py:53
  2.6 0.7 compare_and_fusion
  3.2 0.9 %fusion.19 = f32[4,256]{1,0:T(4,128)S(1)} fusion(bf16[1024,256]{1,0:T(8,128)(2,1)S(1)} %copy-done, bf16[4,1024]{1,0:T(4,128)(2,1)} %param.14, f32[1024]{0:T(1024)} %param.15), kind=kOutput, calls=%fused_computation.48 | convolution fusion | flops 2109440 | bytes 540672 | tf_op jit(solution)/shard_map/dot_general | solution.py:48
  4.1 1.3 %fusion.16 = f32[4,256]{1,0:T(4,128)S(1)} fusion(bf16[1024,256]{1,0:T(8,128)(2,1)} %param.18, bf16[4,1024]{1,0:T(4,128)(2,1)} %param.14, f32[1024]{0:T(1024)} %param.15), kind=kOutput, calls=%fused_computation.47 | convolution fusion | flops 2109440 | bytes 540672 | tf_op jit(solution)/shard_map/dot_general | solution.py:49
  5.5 1.0 %select_reduce_fusion.1 = f32[4,4]{1,0:T(4,128)S(1)} fusion(f32[4,4,2048]{2,1,0:T(4,128)} %param.25, pred[4,2048]{1,0:T(4,128)(4,1)S(1)} %iota_compare_fusion), kind=kLoop, calls=%fused_computation.8 | loop fusion | flops 65520 | bytes 139328 | tf_op jit(solution)/shard_map/reduce_sum | solution.py:80
  6.5 0.7 broadcast_compare_fusion
  7.3 2.9 %fusion.21 = f32[4,2048]{1,0:T(4,128)S(1)} fusion(bf16[1024,2048]{1,0:T(8,128)(2,1)} %param.16, bf16[4,1024]{1,0:T(4,128)(2,1)} %param.14, f32[1024]{0:T(1024)} %param.15), kind=kOutput, calls=%fused_computation.49 | convolution fusion | flops 16789504 | bytes 4239360 | tf_op jit(solution)/shard_map/dot_general | solution.py:47
  10.1 21.3 %all-reduce.1 = (f32[4,2048]{1,0:T(4,128)S(1)}, f32[4]{0:T(128)S(1)}, f32[4,256]{1,0:T(4,128)S(1)}, f32[4,4]{1,0:T(4,128)S(1)}, f32[4,256]{1,0:T(4,128)S(1)}) all-reduce(f32[4,2048]{1,0:T(4,128)S(1)} %fusion.21, f32[4]{0:T(128)S(1)} %fusion.3, f32[4,256]{1,0:T(4,128)S(1)} %fusion.19, ...), channel_id=1, replica_groups=mesh['dp'=4,'kv'=4,'tp'=2] {'kv'}, use_global_device_ids=true, to_apply=%region_0.0 | all-reduce | flops 10260 | bytes 82080 | tf_op jit(solution)/shard_map/psum | solution.py:54
  31.8 0.1 multiply_reduce_fusion.1
  32.0 0.1 reshape.98
  32.1 0.1 multiply_reduce_fusion
  32.2 0.2 fusion.7
  32.4 6.3 %copy.17 = bf16[4,2048,256]{1,2,0:T(8,128)(2,1)} copy(bf16[4,2048,256]{2,1,0:T(8,128)(2,1)} %param.23) | data formatting | bytes 8388608 | tf_op args[9]
  38.8 3.0 %select_reduce_fusion = (f32[4,4,8]{2,1,0:T(4,128)S(1)}, f32[4,4,8,2048]{3,2,1,0:T(8,128)S(1)}) fusion(pred[4,2048]{1,0:T(4,128)(4,1)S(1)} %broadcast_compare_fusion, f32[4,4,2048]{2,1,0:T(4,128)S(1)} %copy-done.1, bf16[4,2048,4,64]{1,3,2,0:T(8,128)(2,1)} %bitcast.15, f32[4,4,8,64]{3,2,1,0:T(8,128)S(1)} %reshape.98, f32[64]{0:T(128)S(1)} %copy-done.2, ...), kind=kOutput, calls=%fused_computation.7 | convolution fusion | flops 34627456 | bytes 5416192 | tf_op jit(solution)/shard_map/sgrd,spgd->sgrp/dot_general | solution.py:72
  41.9 0.4 convert_reduce_fusion
  42.2 8.5 %pmax.7 = f32[4,4,8]{2,1,0:T(4,128)S(1)} all-reduce(f32[4,4,8]{2,1,0:T(4,128)S(1)} %maximum_select_fusion), channel_id=1, replica_groups=mesh['dp'=4,'kv'=4,'tp'=2] {'kv'}, use_global_device_ids=true, to_apply=%region_10.11 | all-reduce | flops 128 | bytes 1024 | tf_op jit(solution)/shard_map/pmax | solution.py:95
  50.8 6.3 %copy.18 = bf16[4,2048,256]{1,2,0:T(8,128)(2,1)} copy(bf16[4,2048,256]{2,1,0:T(8,128)(2,1)} %param.24) | data formatting | bytes 8388608 | tf_op args[10]
  57.1 3.4 %fusion.1 = f32[4,4,8,64]{3,2,1,0:T(8,128)S(1)} fusion(bf16[4,2048,4,64]{1,3,2,0:T(8,128)(2,1)} %bitcast.16, f32[4,4,8,2048]{3,2,1,0:T(8,128)S(1)} %get-tuple-element.20, f32[4,4,8]{2,1,0:T(4,128)S(1)} %maximum_select_fusion, pred[4,2048]{1,0:T(4,128)(4,1)S(1)} %broadcast_compare_fusion, f32[4,4,8]{2,1,0:T(4,128)S(1)} %get-tuple-element.14, ...), kind=kOutput, calls=%fused_computation.3 | convolution fusion | flops 34365440 | bytes 5289472 | tf_op jit(solution)/shard_map/sgrp,spgd->sgrd/dot_general | solution.py:93
  60.5 19.0 %all-reduce = (f32[4,4,8,64]{3,2,1,0:T(8,128)S(1)}, f32[4,4,8]{2,1,0:T(4,128)S(1)}) all-reduce(f32[4,4,8,64]{3,2,1,0:T(8,128)S(1)} %fusion.1, f32[4,4,8]{2,1,0:T(4,128)S(1)} %get-tuple-element.12), channel_id=1, replica_groups=mesh['dp'=4,'kv'=4,'tp'=2] {'kv'}, use_global_device_ids=true, to_apply=%region_11.12 | all-reduce | flops 8320 | bytes 66560 | tf_op jit(solution)/shard_map/psum | solution.py:97
  79.6 0.1 reshape.97
  79.7 2.8 %convolution_convert_fusion = bf16[4,1024]{1,0:T(4,128)(2,1)S(1)} fusion(bf16[4,2048]{1,0:T(4,128)(2,1)S(1)} %reshape.97, bf16[2048,1024]{1,0:T(8,128)(2,1)} %param.27), kind=kOutput, calls=%fused_computation.4 | convolution fusion | flops 16781312 | bytes 4218880 | tf_op jit(solution)/shard_map/dot_general | solution.py:99
  82.5 3.1 %psum.63 = bf16[4,1024]{1,0:T(4,128)(2,1)} all-reduce(bf16[4,1024]{1,0:T(4,128)(2,1)S(1)} %convolution_convert_fusion), channel_id=1, replica_groups=mesh['dp'=4,'kv'=4,'tp'=2] {'tp'}, use_global_device_ids=true, to_apply=%region_14.15 | all-reduce | flops 4096 | bytes 16384 | tf_op jit(solution)/shard_map/psum | solution.py:103
  (22 shorter events, 0.8 us)
Async XLA Ops:
  0.0 3.2 %copy-start = (bf16[1024,256]{1,0:T(8,128)(2,1)S(1)}, bf16[1024,256]{1,0:T(8,128)(2,1)}, u32[]{:S(2)}) copy-start(bf16[1024,256]{1,0:T(8,128)(2,1)} %param.17) | copy-start | bytes 1572868
  0.0 32.2 %copy-start.2 = (f32[64]{0:T(128)S(1)}, f32[64]{0:T(128)}, u32[]{:S(2)}) copy-start(f32[64]{0:T(128)} %param.21) | copy-start | bytes 772
  0.0 31.9 %copy-start.3 = (f32[64]{0:T(128)S(1)}, f32[64]{0:T(128)}, u32[]{:S(2)}) copy-start(f32[64]{0:T(128)} %param.22) | copy-start | bytes 772
  32.4 6.3 %copy-start.1 = (f32[4,4,2048]{2,1,0:T(4,128)S(1)}, f32[4,4,2048]{2,1,0:T(4,128)}, u32[]{:S(2)}) copy-start(f32[4,4,2048]{2,1,0:T(4,128)} %param.25) | copy-start | bytes 393220
where the time goes:
time: 86.3 us; the launch traced here: 85.6 us
  blocking collectives  51.8 us (60%)
  matrix products  15.4 us (18%)
  local copies, waits for them, and re-layouts  13.8 us (16%)
  other arithmetic  4.47 us (5%)
    psum x1, blocking collectives, per_device(): lax.psum((query_part, key_part, value_part, gate_part, squares), 'kv')  21.3 us
    psum x1, blocking collectives, per_device(): lax.psum((totals * factor, weighted * factor[..., None]), 'kv')  19 us
    unnamed x10, local copies, waits for them, and re-layouts  12.6 us
    pmax x1, blocking collectives, per_device(): top = lax.pmax(maxima, 'kv')  8.49 us
    dot_general x1, matrix products, per_device(): jnp.einsum('sgrp,spgd->sgrd', weights, values, preferred_element_type=jnp...  3.42 us
    psum x1, blocking collectives, per_device(): return lax.psum(partial_value.astype(jnp.bfloat16), 'tp')  3.06 us
    dot_general x1, matrix products, per_device(): jnp.einsum('sgrd,spgd->sgrp', queries, keys, preferred_element_type=jnp.f...  3 us
    dot_general x1, matrix products, per_device(): jnp.dot(scaled, query_weight, preferred_element_type=jnp.float32)  2.88 us

commit v1 on v0

v1 whole, which is shorter than its diff:
```python
import functools

import jax
import jax.numpy as jnp
from jax import lax
from jax.experimental import pallas as pl
from jax.experimental.pallas import tpu as pltpu
from jax.sharding import PartitionSpec as P

EPSILON = 1e-06
FLOOR = -1e30
LANES = 128
CHUNKS = 4
MESH = pl.DeviceIdType.MESH
F32 = jnp.float32
BF16 = jnp.bfloat16


def kernel(
    dims,
    tokens,
    norm_gain,
    query_weight,
    key_weight,
    value_weight,
    gate_weight,
    gate_bias,
    query_gain,
    key_gain,
    key_cache,
    value_cache,
    gate_cache,
    lengths,
    out_weight,
    out,
    qw,
    kw,
    vw,
    gw,
    keys,
    values,
    gates,
    ow,
    part,
    bias,
    heads_q,
    heads_o,
    mixed_in,
    sums,
    blocks,
    stats,
    halves,
    local_sem,
    send_sum,
    recv_sum,
    send_block,
    recv_block,
    send_stat,
    recv_stat,
    half_sem,
):
    n_kv, n_tp, width, head = dims
    kv = lax.axis_index("kv")
    tp = lax.axis_index("tp")
    seqs, columns = tokens.shape
    positions = keys.shape[1]
    q_chunk = qw.shape[2]
    q_rows = query_weight.shape[1] // LANES
    k_width = key_weight.shape[1]
    k_rows = k_width // LANES
    groups = k_width // head
    n_heads = query_weight.shape[1] // head
    ratio = n_heads // groups
    k_base = seqs * q_rows
    v_base = k_base + seqs * k_rows
    g_base = v_base + seqs * k_rows
    gate_columns = gate_weight.shape[0]

    barrier = pltpu.get_barrier_semaphore()
    for step in range(1, n_kv):
        peer = lax.rem(kv + step, n_kv)
        pl.semaphore_signal(barrier, inc=1, device_id={"kv": peer}, device_id_type=MESH)
    for step in range(1, n_tp):
        peer = lax.rem(tp + step, n_tp)
        pl.semaphore_signal(barrier, inc=1, device_id={"tp": peer}, device_id_type=MESH)

    loads = []

    def load(src, dst):
        copy = pltpu.make_async_copy(src, dst, local_sem.at[len(loads)])
        copy.start()
        loads.append(copy)
        return copy

    row_start = pl.multiple_of(kv * columns, LANES)
    load_q = [
        load(query_weight.at[:, pl.ds(i * q_chunk, q_chunk)], qw.at[i]) for i in range(CHUNKS)
    ]
    load_k = load(key_weight, kw)
    load_v = load(value_weight, vw)
    load_g = load(gate_weight.at[:, pl.ds(row_start, columns)], gw)
    load_gates = load(gate_cache, gates)
    load_keys = [load(key_cache.at[s], keys.at[s]) for s in range(seqs)]
    load_values = [load(value_cache.at[s], values.at[s]) for s in range(seqs)]
    load_out = load(out_weight, ow)

    tokens_f = tokens[...].astype(F32)
    squares = jnp.sum(tokens_f * tokens_f, axis=1, keepdims=True)
    scaled = (tokens_f * norm_gain[...]).astype(BF16)
    for i in range(CHUNKS):
        load_q[i].wait()
        product = jnp.dot(scaled, qw[i], preferred_element_type=F32)
        for j in range(q_chunk // LANES):
            row = i * (q_chunk // LANES) + j
            part[pl.ds(row, seqs, stride=q_rows), :] = product[:, j * LANES : (j + 1) * LANES]
    for copy, weight, base in ((load_k, kw, k_base), (load_v, vw, v_base)):
        copy.wait()
        product = jnp.dot(scaled, weight[...], preferred_element_type=F32)
        for j in range(k_rows):
            part[pl.ds(base + j, seqs, stride=k_rows), :] = product[:, j * LANES : (j + 1) * LANES]
    load_g.wait()
    part[g_base:, :] = jnp.zeros((part.shape[0] - g_base, LANES), F32)
    part[g_base : g_base + seqs, :gate_columns] = lax.dot_general(
        scaled, gw[...], (((1,), (1,)), ((), ())), preferred_element_type=F32
    )
    part[g_base : g_base + seqs, gate_columns : gate_columns + 1] = squares
    sums[kv] = part[...].astype(BF16)

    pl.semaphore_wait(barrier, n_kv + n_tp - 2)

    def spread(ref, send, recv):
        copies = []
        for step in range(1, n_kv):
            peer = lax.rem(kv + step, n_kv)
            copy = pltpu.make_async_remote_copy(
                src_ref=ref.at[kv],
                dst_ref=ref.at[kv],
                send_sem=send.at[step],
                recv_sem=recv.at[kv],
                device_id={"kv": peer},
                device_id_type=MESH,
            )
            copy.start()
            copies.append(copy)
        return copies

    def arrive(ref, send, recv):
        for step in range(1, n_kv):
            peer = lax.rem(kv + n_kv - step, n_kv)
            pltpu.make_async_remote_copy(
                src_ref=ref.at[peer],
                dst_ref=ref.at[peer],
                send_sem=send.at[step],
                recv_sem=recv.at[peer],
                device_id={"kv": peer},
                device_id_type=MESH,
            ).wait_recv()

    sent = spread(sums, send_sum, recv_sum)

    lane = lax.broadcasted_iota(jnp.int32, (1, LANES), 1)
    low = lane < head
    places = lax.broadcasted_iota(jnp.int32, (groups, positions), 1)
    load_gates.wait()
    last_gates = []
    for s in range(seqs):
        within = lengths[s] - 1 - kv * positions
        gate = gates[s]
        bias[s] = jnp.where(places <= within, -gate, FLOOR)
        last_gates.append(
            jnp.sum(jnp.where(places == within, gate, 0.0), axis=1, keepdims=True)
        )
    bias_row = jnp.zeros((1, LANES), F32)
    for j in range(gate_columns):
        bias_row = jnp.where(lane == j, gate_bias[j], bias_row)
    q_gain = jnp.concatenate([query_gain[...]] * (LANES // head), axis=1)
    k_gain = jnp.concatenate([key_gain[...]] * (LANES // head), axis=1)

    def head_norm(raw, gain):
        square = raw * raw
        first = jnp.sum(jnp.where(low, square, 0.0), axis=1, keepdims=True)
        second = jnp.sum(jnp.where(low, 0.0, square), axis=1, keepdims=True)
        factor = jnp.where(
            low, lax.rsqrt(first / head + EPSILON), lax.rsqrt(second / head + EPSILON)
        )
        return (raw * factor * gain).astype(BF16).astype(F32)

    def swap(x):
        return pltpu.roll(x, head, 1)

    head_row = lax.broadcasted_iota(jnp.int32, (n_heads, k_width), 0)
    head_lane = lax.broadcasted_iota(jnp.int32, (n_heads, k_width), 1)
    own_group = (head_row // ratio) == (head_lane // head)
    stat_row = lax.broadcasted_iota(jnp.int32, (n_heads, LANES), 0)
    stat_lane = lax.broadcasted_iota(jnp.int32, (n_heads, LANES), 1)

    arrive(sums, send_sum, recv_sum)
    total = sums[0].astype(F32)
    for i in range(1, n_kv):
        total = total + sums[i].astype(F32)
    tail = total[g_base : g_base + seqs]
    square_sum = jnp.sum(jnp.where(lane == gate_columns, tail, 0.0), axis=1, keepdims=True)
    inverse = lax.rsqrt(square_sum / width + EPSILON)
    logits = tail * inverse + bias_row
    log_gate = jnp.minimum(logits, 0.0) - jnp.log1p(jnp.exp(-jnp.abs(logits)))

    max_row = jnp.zeros((1, LANES), F32)
    sum_row = jnp.zeros((1, LANES), F32)
    for s in range(seqs):
        inv = inverse[s : s + 1]
        raw = (total[s * q_rows : (s + 1) * q_rows] * inv).astype(BF16).astype(F32)
        query = head_norm(raw, q_gain) * (head ** -0.5)
        turned = swap(query)
        heads_q[s, pl.ds(0, q_rows, stride=2), :] = jnp.where(low, query, turned)
        heads_q[s, pl.ds(1, q_rows, stride=2), :] = jnp.where(low, turned, query)
        key_raw = total[k_base + s * k_rows : k_base + (s + 1) * k_rows] * inv
        key_new = head_norm(key_raw.astype(BF16).astype(F32), k_gain)
        value_new = (
            (total[v_base + s * k_rows : v_base + (s + 1) * k_rows] * inv)
            .astype(BF16)
            .astype(F32)
        )
        key_row = jnp.concatenate([key_new[j : j + 1] for j in range(k_rows)], axis=1)
        value_row = jnp.concatenate([value_new[j : j + 1] for j in range(k_rows)], axis=1)
        spread_q = jnp.where(
            own_group, jnp.concatenate([heads_q[s]] * k_rows, axis=1), 0.0
        )
        score_new = jnp.sum(spread_q * key_row, axis=1, keepdims=True)
        own_gate = []
        for g in range(groups):
            gate = last_gates[s][g : g + 1] + jnp.sum(
                jnp.where(lane == tp * groups + g, log_gate[s : s + 1], 0.0),
                axis=1,
                keepdims=True,
            )
            own_gate.append(jnp.broadcast_to(gate, (ratio, 1)))
        score_new = score_new - jnp.concatenate(own_gate, axis=0)
        within = jnp.full((n_heads, 1), lengths[s] - 1 - kv * positions, jnp.int32)
        owner = (within >= 0) & (within < positions)
        load_keys[s].wait()
        scores = lax.dot_general(
            spread_q.astype(BF16),
            keys[s],
            (((1,), (1,)), ((), ())),
            preferred_element_type=F32,
        )
        scores = scores + jnp.concatenate(
            [jnp.broadcast_to(bias[s, g : g + 1, :], (ratio, positions)) for g in range(groups)],
            axis=0,
        )
        top = jnp.max(scores, axis=1, keepdims=True)
        top = jnp.maximum(top, jnp.where(owner, score_new, FLOOR))
        weights = jnp.exp(scores - top)
        weight_new = jnp.where(owner, jnp.exp(score_new - top), 0.0)
        weight_new = weight_new.astype(BF16).astype(F32)
        block_sum = jnp.sum(weights, axis=1, keepdims=True) + weight_new
        pick = stat_lane == stat_row + s * n_heads
        max_row = max_row + jnp.sum(jnp.where(pick, top, 0.0), axis=0, keepdims=True)
        sum_row = sum_row + jnp.sum(jnp.where(pick, block_sum, 0.0), axis=0, keepdims=True)
        load_values[s].wait()
        found = jnp.dot(weights.astype(BF16), values[s], preferred_element_type=F32)
        found = jnp.where(own_group, found + weight_new * value_row, 0.0)
        folded = found[:, :LANES]
        for j in range(1, k_rows):
            folded = folded + found[:, j * LANES : (j + 1) * LANES]
        heads_o[s] = folded + swap(folded)
        packed = jnp.where(
            low,
            heads_o[s, pl.ds(0, q_rows, stride=2), :],
            heads_o[s, pl.ds(1, q_rows, stride=2), :],
        )
        blocks[kv, s * q_rows : (s + 1) * q_rows, :] = packed.astype(BF16)
    stats[kv, 0:1, :] = max_row
    stats[kv, 1:2, :] = sum_row
    sent += spread(stats, send_stat, recv_stat)
    sent += spread(blocks, send_block, recv_block)

    arrive(stats, send_stat, recv_stat)
    maxima = [stats[i, 0:1, :] for i in range(n_kv)]
    top = functools.reduce(jnp.maximum, maxima)
    factors = [jnp.exp(m - top) for m in maxima]
    normal = functools.reduce(
        jnp.add, [factors[i] * stats[i, 1:2, :] for i in range(n_kv)]
    )
    pair_row = lax.broadcasted_iota(jnp.int32, (seqs * q_rows, LANES), 0)
    pair_lane = lax.broadcasted_iota(jnp.int32, (seqs * q_rows, LANES), 1)
    shares = []
    for i in range(n_kv):
        share = factors[i] / normal
        first = jnp.sum(jnp.where(pair_lane == 2 * pair_row, share, 0.0), axis=1, keepdims=True)
        second = jnp.sum(
            jnp.where(pair_lane == 2 * pair_row + 1, share, 0.0), axis=1, keepdims=True
        )
        shares.append(jnp.where(low, first, second))
    arrive(blocks, send_block, recv_block)
    attended = shares[0] * blocks[0].astype(F32)
    for i in range(1, n_kv):
        attended = attended + shares[i] * blocks[i].astype(F32)
    mixed_in[...] = attended
    flat = jnp.concatenate(
        [mixed_in[pl.ds(c, seqs, stride=q_rows), :] for c in range(q_rows)], axis=1
    ).astype(BF16)
    load_out.wait()
    mixed = jnp.dot(flat, ow[...], preferred_element_type=F32).astype(BF16)
    halves[tp] = mixed
    for step in range(1, n_tp):
        peer = lax.rem(tp + step, n_tp)
        copy = pltpu.make_async_remote_copy(
            src_ref=halves.at[tp],
            dst_ref=halves.at[tp],
            send_sem=half_sem.at[0, step],
            recv_sem=half_sem.at[1, tp],
            device_id={"tp": peer},
            device_id_type=MESH,
        )
        copy.start()
        sent.append(copy)
    for step in range(1, n_tp):
        peer = lax.rem(tp + n_tp - step, n_tp)
        pltpu.make_async_remote_copy(
            src_ref=halves.at[peer],
            dst_ref=halves.at[peer],
            send_sem=half_sem.at[0, step],
            recv_sem=half_sem.at[1, peer],
            device_id={"tp": peer},
            device_id_type=MESH,
        ).wait_recv()
    result = halves[0].astype(F32)
    for i in range(1, n_tp):
        result = result + halves[i].astype(F32)
    out[...] = result.astype(BF16)
    for copy in sent:
        copy.wait_send()


def per_device(
    n_kv,
    n_tp,
    tokens,
    norm_gain,
    query_weight,
    key_weight,
    value_weight,
    gate_weight,
    gate_bias,
    query_gain,
    key_gain,
    key_cache,
    value_cache,
    gate_cache,
    lengths,
    out_weight,
):
    seqs, columns = tokens.shape
    head = query_gain.shape[0]
    q_width = query_weight.shape[1]
    k_width = key_weight.shape[1]
    n_heads = q_width // head
    q_rows, k_rows = q_width // LANES, k_width // LANES
    used = seqs * (q_rows + 2 * k_rows + 1)
    rows = -(-used // 16) * 16
    any_space = pl.BlockSpec(memory_space=pl.ANY)
    vmem = pl.BlockSpec(memory_space=pltpu.VMEM)
    smem = pl.BlockSpec(memory_space=pltpu.SMEM)
    dma = pltpu.SemaphoreType.DMA
    copies = CHUNKS + 5 + 2 * seqs
    call = pl.pallas_call(
        functools.partial(kernel, (n_kv, n_tp, gate_weight.shape[0], head)),
        out_shape=jax.ShapeDtypeStruct((seqs, out_weight.shape[1]), BF16),
        in_specs=[
            vmem,
            vmem,
            any_space,
            any_space,
            any_space,
            any_space,
            smem,
            vmem,
            vmem,
            any_space,
            any_space,
            any_space,
            smem,
            any_space,
        ],
        out_specs=vmem,
        scratch_shapes=[
            pltpu.VMEM((CHUNKS, columns, q_width // CHUNKS), BF16),
            pltpu.VMEM((columns, k_width), BF16),
            pltpu.VMEM((columns, k_width), BF16),
            pltpu.VMEM((gate_weight.shape[1], columns), BF16),
            pltpu.VMEM(key_cache.shape, BF16),
            pltpu.VMEM(value_cache.shape, BF16),
            pltpu.VMEM(gate_cache.shape, F32),
            pltpu.VMEM(out_weight.shape, BF16),
            pltpu.VMEM((rows, LANES), F32),
            pltpu.VMEM(gate_cache.shape, F32),
            pltpu.VMEM((seqs, n_heads, LANES), F32),
            pltpu.VMEM((seqs, n_heads, LANES), F32),
            pltpu.VMEM((seqs * q_rows, LANES), F32),
            pltpu.VMEM((n_kv, rows, LANES), BF16),
            pltpu.VMEM((n_kv, seqs * q_rows, LANES), BF16),
            pltpu.VMEM((n_kv, 2, LANES), F32),
            pltpu.VMEM((n_tp, seqs, out_weight.shape[1]), BF16),
            dma((copies,)),
            dma((n_kv,)),
            dma((n_kv,)),
            dma((n_kv,)),
            dma((n_kv,)),
            dma((n_kv,)),
            dma((n_kv,)),
            dma((2, n_tp)),
        ],
        compiler_params=pltpu.CompilerParams(
            collective_id=0, has_side_effects=True, vmem_limit_bytes=60 * 1024 * 1024
        ),
    )
    return call(
        tokens,
        norm_gain.reshape(1, columns),
        query_weight,
        key_weight,
        value_weight,
        gate_weight.T,
        gate_bias,
        query_gain.reshape(1, head),
        key_gain.reshape(1, head),
        key_cache,
        value_cache,
        gate_cache,
        lengths,
        out_weight,
    )


def solution(mesh):
    return jax.shard_map(
        functools.partial(per_device, mesh.shape["kv"], mesh.shape["tp"]),
        mesh=mesh,
        in_specs=(
            P("dp", "kv"),
            P("kv"),
            P("kv", "tp"),
            P("kv", "tp"),
            P("kv", "tp"),
            P(),
            P(),
            P(),
            P(),
            P("dp", "kv", "tp"),
            P("dp", "kv", "tp"),
            P("dp", "tp", "kv"),
            P("dp"),
            P("tp", "kv"),
        ),
        out_specs=P("dp", "kv"),
        check_vma=False,
    )
```

time: 86.3 us -> 23.9 us (0.28)
  blocking collectives: 51.8 us -> 0 us
  Pallas kernels: 0 us -> 22.3 us
  matrix products: 15.4 us -> 0 us
  local copies, waits for them, and re-layouts: 13.8 us -> 1.3 us
  other arithmetic: 4.47 us -> 0 us
    psum x3 -> x0, blocking collectives: 43.3 us -> none  [the longest x1 21.3 us: per_device(): lax.psum((query_part, key_part, value_part, gate_part, squares), 'kv')]
    pallas_call x0 -> x1, Pallas kernels: none -> 22.3 us  [per_device(): call(tokens, norm_gain.reshape(1, columns), query_weight, key_weight, val...]
    dot_general x8 -> x0, matrix products: 15.4 us -> none  [the longest x1 3.42 us: per_device(): jnp.einsum('sgrp,spgd->sgrd', weights, values, preferred_element_type=jnp...]
    unnamed x10 -> x1, local copies, waits for them, and re-layouts: 12.6 us -> 1.3 us
    pmax x1 -> x0, blocking collectives: 8.49 us -> none  [per_device(): top = lax.pmax(maxima, 'kv')]
    reduce_sum x5 -> x0, other arithmetic: 2.41 us -> none  [the longest x1 1.04 us: per_device(): last_gate = jnp.sum(jnp.where(picked, gate_cache, 0.0), axis=2)]
where the time goes in v1:
time: 23.9 us; the launch traced here: 23.6 us
  Pallas kernels  22.3 us (93%)
  local copies, waits for them, and re-layouts  1.3 us (5%)
    pallas_call x1, Pallas kernels, per_device(): call(tokens, norm_gain.reshape(1, columns), query_weight, key_weight, val...  22.3 us
    unnamed x1, local copies, waits for them, and re-layouts  1.3 us

profile of v1, /device:TPU:0, one launch (start us, length us, event | category | flops | bytes accessed | tf_op | source)
XLA Modules:
  0.0 23.6 jit_solution(5154642460793645782)
XLA Ops:
  0.0 22.3 %shard_map.136 = bf16[4,1024]{1,0:T(4,128)(2,1)} custom-call(bf16[4,1024]{1,0:T(4,128)(2,1)} %tokens.1, f32[1,1024]{1,0:T(1,128)} %bitcast.5, bf16[1024,2048]{1,0:T(8,128)(2,1)} %query_weight.1, bf16[1024,256]{1,0:T(8,128)(2,1)} %key_weight.1, bf16[1024,256]{1,0:T(8,128)(2,1)} %value_weight.1, bf16[8,4096]{1,0:T(8,128)(2,1)} %bitcast.4, f32[8]{0:T(128)} %gate_bias.1, ...), custom_call_target="tpu_custom_call" | custom-call | tf_op jit(solution)/shard_map/pallas_call | solution.py:418
  22.3 1.3 %copy.16 = bf16[4,1024]{1,0:T(4,128)(2,1)} copy(bf16[4,1024]{1,0:T(4,128)(2,1)} %shard_map.136) | data formatting | bytes 16384

commit v2 on v1

--- a/solution.py
+++ b/solution.py
@@ -18,21 +18,27 @@
 
 def kernel(
     dims,
-    tokens,
-    norm_gain,
+    tokens_hbm,
+    norm_gain_hbm,
     query_weight,
     key_weight,
     value_weight,
     gate_weight,
+    gate_bias_hbm,
+    query_gain_hbm,
+    key_gain_hbm,
+    key_cache,
+    value_cache,
+    gate_cache,
+    lengths_hbm,
+    out_weight,
+    out,
+    tokens,
+    norm_gain,
     gate_bias,
     query_gain,
     key_gain,
-    key_cache,
-    value_cache,
-    gate_cache,
     lengths,
-    out_weight,
-    out,
     qw,
     kw,
     vw,
@@ -92,6 +98,14 @@
         loads.append(copy)
         return copy
 
+    small = [
+        load(tokens_hbm, tokens),
+        load(norm_gain_hbm, norm_gain),
+        load(lengths_hbm, lengths),
+        load(gate_bias_hbm, gate_bias),
+        load(query_gain_hbm, query_gain),
+        load(key_gain_hbm, key_gain),
+    ]
     row_start = pl.multiple_of(kv * columns, LANES)
     load_q = [
         load(query_weight.at[:, pl.ds(i * q_chunk, q_chunk)], qw.at[i]) for i in range(CHUNKS)
@@ -104,6 +118,8 @@
     load_values = [load(value_cache.at[s], values.at[s]) for s in range(seqs)]
     load_out = load(out_weight, ow)
 
+    for copy in small:
+        copy.wait()
     tokens_f = tokens[...].astype(F32)
     squares = jnp.sum(tokens_f * tokens_f, axis=1, keepdims=True)
     scaled = (tokens_f * norm_gain[...]).astype(BF16)
@@ -194,6 +210,8 @@
     stat_row = lax.broadcasted_iota(jnp.int32, (n_heads, LANES), 0)
     stat_lane = lax.broadcasted_iota(jnp.int32, (n_heads, LANES), 1)
 
+    for copy in load_keys + load_values + [load_out]:
+        copy.wait()
     arrive(sums, send_sum, recv_sum)
     total = sums[0].astype(F32)
     for i in range(1, n_kv):
@@ -237,7 +255,6 @@
         score_new = score_new - jnp.concatenate(own_gate, axis=0)
         within = jnp.full((n_heads, 1), lengths[s] - 1 - kv * positions, jnp.int32)
         owner = (within >= 0) & (within < positions)
-        load_keys[s].wait()
         scores = lax.dot_general(
             spread_q.astype(BF16),
             keys[s],
@@ -257,7 +274,6 @@
         pick = stat_lane == stat_row + s * n_heads
         max_row = max_row + jnp.sum(jnp.where(pick, top, 0.0), axis=0, keepdims=True)
         sum_row = sum_row + jnp.sum(jnp.where(pick, block_sum, 0.0), axis=0, keepdims=True)
-        load_values[s].wait()
         found = jnp.dot(weights.astype(BF16), values[s], preferred_element_type=F32)
         found = jnp.where(own_group, found + weight_new * value_row, 0.0)
         folded = found[:, :LANES]
@@ -300,7 +316,6 @@
     flat = jnp.concatenate(
         [mixed_in[pl.ds(c, seqs, stride=q_rows), :] for c in range(q_rows)], axis=1
     ).astype(BF16)
-    load_out.wait()
     mixed = jnp.dot(flat, ow[...], preferred_element_type=F32).astype(BF16)
     halves[tp] = mixed
     for step in range(1, n_tp):
@@ -359,32 +374,21 @@
     q_rows, k_rows = q_width // LANES, k_width // LANES
     used = seqs * (q_rows + 2 * k_rows + 1)
     rows = -(-used // 16) * 16
-    any_space = pl.BlockSpec(memory_space=pl.ANY)
     vmem = pl.BlockSpec(memory_space=pltpu.VMEM)
-    smem = pl.BlockSpec(memory_space=pltpu.SMEM)
     dma = pltpu.SemaphoreType.DMA
-    copies = CHUNKS + 5 + 2 * seqs
+    copies = CHUNKS + 11 + 2 * seqs
     call = pl.pallas_call(
         functools.partial(kernel, (n_kv, n_tp, gate_weight.shape[0], head)),
-        out_shape=jax.ShapeDtypeStruct((seqs, out_weight.shape[1]), BF16),
-        in_specs=[
-            vmem,
-            vmem,
-            any_space,
-            any_space,
-            any_space,
-            any_space,
-            smem,
-            vmem,
-            vmem,
-            any_space,
-            any_space,
-            any_space,
-            smem,
-            any_space,
-        ],
+        out_shape=pltpu.VMEM((seqs, out_weight.shape[1]), BF16),
+        in_specs=[pl.BlockSpec(memory_space=pltpu.HBM)] * 14,
         out_specs=vmem,
         scratch_shapes=[
+            pltpu.VMEM((seqs, columns), BF16),
+            pltpu.VMEM((1, columns), F32),
+            pltpu.SMEM(gate_bias.shape, F32),
+            pltpu.VMEM((1, head), F32),
+            pltpu.VMEM((1, head), F32),
+            pltpu.SMEM(lengths.shape, jnp.int32),
             pltpu.VMEM((CHUNKS, columns, q_width // CHUNKS), BF16),
             pltpu.VMEM((columns, k_width), BF16),
             pltpu.VMEM((columns, k_width), BF16),

time: 23.9 us -> 19.3 us (0.81)
  Pallas kernels: 22.3 us -> 18.5 us
  local copies, waits for them, and re-layouts: 1.3 us -> 0.6 us
    pallas_call x1, Pallas kernels: 22.3 us -> 18.5 us  [per_device(): call(tokens, norm_gain.reshape(1, columns), query_weight, key_weight, val...]
    unnamed x1, local copies, waits for them, and re-layouts: 1.3 us -> 0.6 us
where the time goes in v2:
time: 19.3 us; the launch traced here: 19.1 us
  Pallas kernels  18.5 us (96%)
  local copies, waits for them, and re-layouts  0.6 us (3%)
    pallas_call x1, Pallas kernels, per_device(): call(tokens, norm_gain.reshape(1, columns), query_weight, key_weight, val...  18.5 us
    unnamed x1, local copies, waits for them, and re-layouts  0.6 us

profile of v2, /device:TPU:0, one launch (start us, length us, event | category | flops | bytes accessed | tf_op | source)
XLA Modules:
  0.0 19.1 jit_solution(7487364720235003638)
XLA Ops:
  0.0 18.5 %shard_map.136 = bf16[4,1024]{1,0:T(4,128)(2,1)S(1)} custom-call(bf16[4,1024]{1,0:T(4,128)(2,1)} %tokens_hbm.1, f32[1,1024]{1,0:T(1,128)} %bitcast.5, bf16[1024,2048]{1,0:T(8,128)(2,1)} %query_weight.1, bf16[1024,256]{1,0:T(8,128)(2,1)} %key_weight.1, bf16[1024,256]{1,0:T(8,128)(2,1)} %value_weight.1, bf16[8,4096]{1,0:T(8,128)(2,1)} %bitcast.4, ...), custom_call_target="tpu_custom_call" | custom-call | tf_op jit(solution)/shard_map/pallas_call | solution.py:422
  18.5 0.6 %copy.16 = bf16[4,1024]{1,0:T(4,128)(2,1)} copy(bf16[4,1024]{1,0:T(4,128)(2,1)S(1)} %shard_map.136) | data formatting | bytes 16384

commit v3 on v2

--- a/solution.py
+++ b/solution.py
@@ -56,6 +56,7 @@
     blocks,
     stats,
     halves,
+    turned_keys,
     local_sem,
     send_sum,
     recv_sum,
@@ -144,10 +145,17 @@
 
     pl.semaphore_wait(barrier, n_kv + n_tp - 2)
 
+    def far_first(step):
+        down = n_kv - 1 - step
+        down = down - 1 + (down - kv + n_kv - 1) // n_kv
+        up = step + (step - kv + n_kv) // n_kv
+        upper = (2 * kv) // n_kv
+        return down + upper * (up - down)
+
     def spread(ref, send, recv):
         copies = []
-        for step in range(1, n_kv):
-            peer = lax.rem(kv + step, n_kv)
+        for step in range(n_kv - 1):
+            peer = far_first(step)
             copy = pltpu.make_async_remote_copy(
                 src_ref=ref.at[kv],
                 dst_ref=ref.at[kv],
@@ -212,6 +220,8 @@
 
     for copy in load_keys + load_values + [load_out]:
         copy.wait()
+    for s in range(seqs):
+        turned_keys[s] = keys[s].T
     arrive(sums, send_sum, recv_sum)
     total = sums[0].astype(F32)
     for i in range(1, n_kv):
@@ -255,11 +265,8 @@
         score_new = score_new - jnp.concatenate(own_gate, axis=0)
         within = jnp.full((n_heads, 1), lengths[s] - 1 - kv * positions, jnp.int32)
         owner = (within >= 0) & (within < positions)
-        scores = lax.dot_general(
-            spread_q.astype(BF16),
-            keys[s],
-            (((1,), (1,)), ((), ())),
-            preferred_element_type=F32,
+        scores = jnp.dot(
+            spread_q.astype(BF16), turned_keys[s], preferred_element_type=F32
         )
         scores = scores + jnp.concatenate(
             [jnp.broadcast_to(bias[s, g : g + 1, :], (ratio, positions)) for g in range(groups)],
@@ -373,7 +380,7 @@
     n_heads = q_width // head
     q_rows, k_rows = q_width // LANES, k_width // LANES
     used = seqs * (q_rows + 2 * k_rows + 1)
-    rows = -(-used // 16) * 16
+    rows = -(-used // 8) * 8
     vmem = pl.BlockSpec(memory_space=pltpu.VMEM)
     dma = pltpu.SemaphoreType.DMA
     copies = CHUNKS + 11 + 2 * seqs
@@ -406,6 +413,7 @@
             pltpu.VMEM((n_kv, seqs * q_rows, LANES), BF16),
             pltpu.VMEM((n_kv, 2, LANES), F32),
             pltpu.VMEM((n_tp, seqs, out_weight.shape[1]), BF16),
+            pltpu.VMEM((seqs, key_cache.shape[2], key_cache.shape[1]), BF16),
             dma((copies,)),
             dma((n_kv,)),
             dma((n_kv,)),

time: 19.3 us -> 19.1 us (0.990)
  Pallas kernels: 18.5 us -> 18.3 us
where the time goes in v3:
time: 19.1 us; the launch traced here: 18.9 us
  Pallas kernels  18.3 us (96%)
  local copies, waits for them, and re-layouts  0.6 us (3%)
    pallas_call x1, Pallas kernels, per_device(): call(tokens, norm_gain.reshape(1, columns), query_weight, key_weight, val...  18.3 us
    unnamed x1, local copies, waits for them, and re-layouts  0.6 us

profile of v3, /device:TPU:0, one launch (start us, length us, event | category | flops | bytes accessed | tf_op | source)
XLA Modules:
  0.0 18.9 jit_solution(359464547169202282)
XLA Ops:
  0.0 18.3 %shard_map.136 = bf16[4,1024]{1,0:T(4,128)(2,1)S(1)} custom-call(bf16[4,1024]{1,0:T(4,128)(2,1)} %tokens_hbm.1, f32[1,1024]{1,0:T(1,128)} %bitcast.5, bf16[1024,2048]{1,0:T(8,128)(2,1)} %query_weight.1, bf16[1024,256]{1,0:T(8,128)(2,1)} %key_weight.1, bf16[1024,256]{1,0:T(8,128)(2,1)} %value_weight.1, bf16[8,4096]{1,0:T(8,128)(2,1)} %bitcast.4, ...), custom_call_target="tpu_custom_call" | custom-call | tf_op jit(solution)/shard_map/pallas_call | solution.py:430
  18.3 0.6 %copy.16 = bf16[4,1024]{1,0:T(4,128)(2,1)} copy(bf16[4,1024]{1,0:T(4,128)(2,1)S(1)} %shard_map.136) | data formatting | bytes 16384
